TPU v7x, 512 devices: a 4x2x32 block of a 4x8x32 slice. The times are simulated.
512 devices in a mesh: grp: 2 (over y), fs: 32 (over z), tp: 8 (over x, core).
Axes of the slice: x: 4, y: 2, z: 32, core: 2. Of those that a mesh axis runs over, the one named last changes fastest.
The devices are a block of a 4x8x32 slice.
Arguments:
- tokens: bfloat16 [12288, 2048], P(('grp', 'fs'), 'tp'), parts along dimension 0, may hold values from -40 to 40
- routes: int32 [12288, 8], P(('grp', 'fs')), parts along dimension 0, may hold values from 0 to 31, all different within a row; in each aligned block of 192 rows (0 to 191, 192 to 383, ...) at most 56 rows name the same one
- routing_weight: float32 [12288, 8], P(('grp', 'fs')), parts along dimension 0, may hold values from 0.1 to 0.6
- norm_gain_vector: float32 [2048], P('tp'), may hold values from 0.1 to 1.9
- expert_gate: float32 [32, 512, 2048], P(None, 'fs', 'tp'), may hold values from -0.125 to 0.125
- expert_up: float32 [32, 512, 2048], P(None, 'fs', 'tp'), may hold values from -0.125 to 0.125
- expert_down: float32 [32, 512, 2048], P(None, 'fs', 'tp'), may hold values from -0.25 to 0.25
- shared_gate: float32 [512, 2048], P('fs', 'tp'), may hold values from -0.125 to 0.125
- shared_up: float32 [512, 2048], P('fs', 'tp'), may hold values from -0.125 to 0.125
- shared_down: float32 [512, 2048], P('fs', 'tp'), may hold values from -0.25 to 0.25
Outputs:
- mixed: bfloat16 [12288, 2048], P(('grp', 'fs'), 'tp'), parts along dimension 0
- gate_served: bfloat16 [64, 512, 2048], P(('grp', 'fs'), None, 'tp'), parts along dimension 0
- up_served: bfloat16 [64, 512, 2048], P(('grp', 'fs'), None, 'tp'), parts along dimension 0
- down_served: bfloat16 [64, 512, 2048], P(('grp', 'fs'), None, 'tp'), parts along dimension 0
- shared_gate_served: bfloat16 [1024, 2048], P('grp', 'tp'), parts along dimension 0
- shared_up_served: bfloat16 [1024, 2048], P('grp', 'tp'), parts along dimension 0
- shared_down_served: bfloat16 [1024, 2048], P('grp', 'tp'), parts along dimension 0
There are 2 independent parts, one for each index of `grp`. A program takes and returns all parts, laid end to end along the dimension named above; an argument that names none is the same for every part. Nothing has to cross between parts.
Inputs may be any that keep to these rules, and one draw needn't show every extreme that they name: `routes`: each row names 8 different experts. In each aligned block of 192 rows no expert is named by more than 56 rows, and in some block an expert is named by exactly 56 rows.
All inputs are finite; a program needn't handle non-finite values.
Results may differ from a plain program's by a relative error of at most 0.022.
Values may be sent and summed in bfloat16 or wider, within the bound.
No kernel may reach another device: no remote copies, remote signals or barrier semaphores. Data moves between devices by JAX's collectives and lax.ppermute only.
A program may use at most 64 MiB of HBM per device.

v0:
```python
import jax
import jax.numpy as jnp
from jax import lax
from jax.sharding import PartitionSpec as P

norm_eps = 1e-06


def sent_together(arrays, axis, split_dim, concat_dim, along):
    widths = [a.shape[along] for a in arrays]
    both = jnp.concatenate(arrays, axis=along)
    out = lax.all_to_all(both, axis, split_axis=split_dim, concat_axis=concat_dim, tiled=True)
    return tuple(jnp.split(out, [sum(widths[:k]) for k in range(1, len(widths))], axis=along))


def sent_together_2(arrays, axis, dim, along):
    both = jnp.concatenate(arrays, axis=along)
    out, at, outs = (lax.all_gather(both, axis, axis=dim, tiled=True), 0, [])
    for a in arrays:
        outs.append(lax.slice_in_dim(out, at, at + a.shape[along], axis=along))
        at += a.shape[along]
    return tuple(outs)


def in_one_piece(arrays, axis, dim, along):
    both = jnp.concatenate(arrays, axis=along)
    out, at, outs = (lax.psum_scatter(both, axis, scatter_dimension=dim, tiled=True), 0, [])
    for a in arrays:
        outs.append(lax.slice_in_dim(out, at, at + a.shape[along], axis=along))
        at += a.shape[along]
    return tuple(outs)


def dense_rows(rows, weight):
    return lax.dot_general(
        rows, weight, (((1,), (1,)), ((), ())), preferred_element_type=jnp.float32
    )


def per_device(
    tokens,
    routes,
    routing_weight,
    norm_gain_vector,
    expert_gate,
    expert_up,
    expert_down,
    shared_gate,
    shared_up,
    shared_down,
):
    tok_rows, portion_width = tokens.shape
    model_width = portion_width * lax.axis_size("tp")
    experts = expert_gate.shape[0]
    top_count = routes.shape[1]
    capacity = tok_rows * top_count * 7 // (6 * experts)
    gate_round = (expert_gate * norm_gain_vector[None, None, :]).astype(jnp.bfloat16)
    up_round = (expert_up * norm_gain_vector[None, None, :]).astype(jnp.bfloat16)
    down_round = expert_down.astype(jnp.bfloat16)
    gate_refreshed, up_new, down_new = sent_together(
        (gate_round, up_round, down_round), "fs", 0, 1, 2
    )
    shared_g, shared_u, shared_d = sent_together_2(
        (
            (shared_gate * norm_gain_vector[None, :]).astype(jnp.bfloat16),
            (shared_up * norm_gain_vector[None, :]).astype(jnp.bfloat16),
            shared_down.astype(jnp.bfloat16),
        ),
        "fs",
        0,
        1,
    )
    values = tokens.astype(jnp.float32)
    totals = lax.psum(jnp.sum(values * values, axis=1), "tp")
    normed = (values * lax.rsqrt(totals / model_width + norm_eps)[:, None]).astype(jnp.bfloat16)
    flat_expert = routes.reshape(-1)
    onehot = (flat_expert[:, None] == jnp.arange(experts, dtype=jnp.int32)[None, :]).astype(
        jnp.int32
    )
    earlier = jnp.cumsum(onehot, axis=0) - onehot
    slot_index = jnp.sum(earlier * onehot, axis=1)
    target = (flat_expert * capacity + slot_index).reshape(tok_rows, top_count)
    places = jnp.arange(experts * capacity, dtype=jnp.int32)
    placing = jnp.sum(
        (target[:, :, None] == places[None, None, :]).astype(jnp.int32), axis=1
    ).astype(jnp.bfloat16)
    outgoing = lax.dot_general(
        placing, normed, (((0,), (0,)), ((), ())), preferred_element_type=jnp.float32
    ).astype(jnp.bfloat16)
    incoming = lax.all_to_all(
        outgoing.reshape(experts, capacity, portion_width),
        "fs",
        split_axis=0,
        concat_axis=0,
        tiled=True,
    )
    arrived = incoming.reshape(experts * capacity, portion_width)
    partials = (
        dense_rows(arrived, gate_refreshed[0]).astype(jnp.bfloat16),
        dense_rows(arrived, up_new[0]).astype(jnp.bfloat16),
        dense_rows(normed, shared_g).astype(jnp.bfloat16),
        dense_rows(normed, shared_u).astype(jnp.bfloat16),
    )
    gate_part, up_part, sgate_part, sup_part = tuple(
        (
            part.astype(jnp.float32)
            for part in in_one_piece(
                (partials[0], partials[1], partials[2], partials[3]), "tp", 1, 0
            )
        )
    )
    hidden, shared_hidden = (
        lax.all_gather(
            (jax.nn.silu(gate_part) * up_part).astype(jnp.bfloat16), "tp", axis=1, tiled=True
        ),
        lax.all_gather(
            (jax.nn.silu(sgate_part) * sup_part).astype(jnp.bfloat16), "tp", axis=1, tiled=True
        ),
    )
    produced = jnp.dot(hidden, down_new[0], preferred_element_type=jnp.float32).astype(jnp.bfloat16)
    returned = lax.all_to_all(
        produced.reshape(experts, capacity, portion_width),
        "fs",
        split_axis=0,
        concat_axis=0,
        tiled=True,
    )
    picked = returned.reshape(experts * capacity, portion_width)[target]
    routed = jnp.sum(routing_weight[:, :, None] * picked.astype(jnp.float32), axis=1)
    shared_out = jnp.dot(shared_hidden, shared_d, preferred_element_type=jnp.float32)
    mixed = (routed + shared_out).astype(jnp.bfloat16)
    return (mixed, gate_refreshed, up_new, down_new, shared_g, shared_u, shared_d)


def solution(mesh):
    return jax.shard_map(
        per_device,
        mesh=mesh,
        in_specs=(
            P(("grp", "fs"), "tp"),
            P(("grp", "fs"), None),
            P(("grp", "fs"), None),
            P("tp"),
            P(None, "fs", "tp"),
            P(None, "fs", "tp"),
            P(None, "fs", "tp"),
            P("fs", "tp"),
            P("fs", "tp"),
            P("fs", "tp"),
        ),
        out_specs=(
            P(("grp", "fs"), "tp"),
            P(("grp", "fs"), None, "tp"),
            P(("grp", "fs"), None, "tp"),
            P(("grp", "fs"), None, "tp"),
            P("grp", "tp"),
            P("grp", "tp"),
            P("grp", "tp"),
        ),
        check_vma=False,
    )
```

profile of v0, /device:TPU:33, one launch (start us, length us, event | category | flops | bytes accessed | tf_op | source)
XLA Modules:
  0.0 525.0 jit_solution(1667189688354686824)
XLA Ops:
  7.2 1.1 convert_element_type.88
  8.3 1.3 multiply_convert_fusion.1
  9.6 1.0 pad_maximum_fusion.1
  10.6 46.3 %all-to-all-start.1 = ((bf16[32,16,768]{2,1,0:T(8,128)(2,1)}), bf16[32,16,768]{2,1,0:T(8,128)(2,1)S(1)}, u32[]{:S(2)}, u32[]{:S(2)}) async-start(bf16[32,16,768]{2,1,0:T(8,128)(2,1)} %pad_maximum_fusion.1), calls=%async_computation.1 | async-start | bytes 1572864 | tf_op jit(solution)/shard_map/all_to_all | solution.py:12
  57.3 9.1 %reduce-window.6 = s32[32,12,128]{2,1,0:T(8,128)S(1)} reduce-window(s32[32,12,128]{2,1,0:T(8,128)S(1)} %fusion.11, s32[]{:T(128)} %constant.6.clone.1), window={size=1x1x128 pad=0_0x0_0x127_0}, to_apply=%region_0.0 | reduce-window | flops 6242304 | bytes 393220 | tf_op jit(solution)/shard_map/reduce-window
  66.5 0.2 copy.47
  66.8 0.1 broadcast_add_fusion
  67.5 13.3 %psum.7 = f32[192]{0:T(256)S(1)} all-reduce(f32[192]{0:T(256)S(1)} %fusion.12), channel_id=1, replica_groups=mesh['grp'=2,'fs'=32,'tp'=8] {'tp'}, use_global_device_ids=true, to_apply=%region_5.6 | all-reduce | flops 192 | bytes 1536 | tf_op jit(solution)/shard_map/psum | solution.py:74
  80.8 5.0 convert_reduce_fusion
  85.9 1.5 convolution_convert_fusion.3
  87.3 55.5 %all-to-all-done.1 = bf16[32,16,768]{2,1,0:T(8,128)(2,1)S(1)} async-done(((bf16[32,16,768]{2,1,0:T(8,128)(2,1)}), bf16[32,16,768]{2,1,0:T(8,128)(2,1)S(1)}, u32[]{:S(2)}, u32[]{:S(2)}) %all-to-all-start.1) | async-done | bytes 786464 | tf_op jit(solution)/shard_map/all_to_all | solution.py:12
  142.8 4.8 all-to-all-start
  147.8 122.6 %all_gather.9 = bf16[512,768]{1,0:T(8,128)(2,1)S(1)} all-gather(bf16[16,768]{1,0:T(8,128)(2,1)S(1)} %pad_maximum_fusion.2), channel_id=1, replica_groups=mesh['grp'=2,'fs'=32,'tp'=8] {'fs'}, dimensions={0}, use_global_device_ids=true | all-gather | bytes 811008 | tf_op jit(solution)/shard_map/all_gather | solution.py:18
  270.5 0.2 convolution_convert_fusion.4
  270.7 0.9 convolution_convert_fusion.5
  271.8 0.7 convolution_convert_fusion
  272.5 0.7 convolution_convert_fusion.1
  273.2 0.2 copy-done.6
  273.4 2.1 pad_maximum_fusion
  275.5 6.3 %copy.56 = bf16[3968,512]{0,1:T(8,128)(2,1)} copy(bf16[3968,512]{1,0:T(8,128)(2,1)} %pad_maximum_fusion) | data formatting | bytes 8126464
  281.8 0.2 all-gather.2.cloned.1.call-start
  282.1 64.3 %reduce-scatter.4.cloned.1.call-done = bf16[64,3968]{1,0:T(8,128)(2,1)} async-done(((bf16[512,3968]{1,0:T(8,128)(2,1)}), bf16[64,3968]{1,0:T(8,128)(2,1)}) %reduce-scatter.4.cloned.1.call-update) | async-done | bytes 507920
  346.4 1.9 fusion.7
  348.3 41.7 %all-gather.2.cloned.1.call-done = bf16[1792,512]{0,1:T(8,128)(2,1)} async-done(((bf16[1792,64]{0,1:T(8,128)(2,1)}), bf16[1792,512]{0,1:T(8,128)(2,1)}) %all-gather.2.cloned.1.call-update) | async-done | bytes 1835024 | tf_op jit(solution)/shard_map/all_gather | solution.py:113
  390.0 3.1 convolution_convert_fusion.2
  393.1 23.3 %all-to-all-start.2 = ((bf16[32,56,256]{2,1,0:T(8,128)(2,1)}), bf16[32,56,256]{2,1,0:T(8,128)(2,1)S(1)}, u32[]{:S(2)}, u32[]{:S(2)}) async-start(bf16[32,56,256]{2,1,0:T(8,128)(2,1)} %bitcast.8), calls=%async_computation.2 | async-start | bytes 1835008 | tf_op jit(solution)/shard_map/all_to_all | solution.py:121
  416.8 0.9 fusion.21
  417.7 13.4 %all_gather.11 = bf16[192,512]{0,1:T(8,128)(2,1)S(1)} all-gather(bf16[192,64]{0,1:T(8,128)(2,1)S(1)} %fusion.21), channel_id=1, replica_groups=mesh['grp'=2,'fs'=32,'tp'=8] {'tp'}, dimensions={1}, use_global_device_ids=true | all-gather | bytes 221184 | tf_op jit(solution)/shard_map/all_gather | solution.py:116
  431.2 80.7 %all-to-all-done.2 = bf16[32,56,256]{2,1,0:T(8,128)(2,1)S(1)} async-done(((bf16[32,56,256]{2,1,0:T(8,128)(2,1)}), bf16[32,56,256]{2,1,0:T(8,128)(2,1)S(1)}, u32[]{:S(2)}, u32[]{:S(2)}) %all-to-all-start.2) | async-done | bytes 917536 | tf_op jit(solution)/shard_map/all_to_all | solution.py:121
  511.9 4.8 gather_fusion
  516.7 0.5 fusion
  517.2 0.9 fusion.1
  (54 shorter events, 1.8 us)
Async XLA Ops:
  9.6 47.3 %copy-start.8 = (s32[192,8]{0,1:T(8,128)S(1)}, s32[192,8]{0,1:T(8,128)}, u32[]{:S(2)}) copy-start(s32[192,8]{0,1:T(8,128)} %param.11) | copy-start | bytes 18436
  10.6 132.3 %all-to-all-start.1 = ((bf16[32,16,768]{2,1,0:T(8,128)(2,1)}), bf16[32,16,768]{2,1,0:T(8,128)(2,1)S(1)}, u32[]{:S(2)}, u32[]{:S(2)}) async-start(bf16[32,16,768]{2,1,0:T(8,128)(2,1)} %pad_maximum_fusion.1), calls=%async_computation.1 | async-start | bytes 1572864 | tf_op jit(solution)/shard_map/all_to_all | solution.py:12
  56.9 10.4 %copy-start = (bf16[192,256]{1,0:T(8,128)(2,1)S(1)}, bf16[192,256]{1,0:T(8,128)(2,1)}, u32[]{:S(2)}) copy-start(bf16[192,256]{1,0:T(8,128)(2,1)} %param.10) | copy-start | bytes 294916
  85.8 61.9 %copy-start.11 = (f32[16,256]{1,0:T(8,128)S(1)}, f32[16,256]{1,0:T(8,128)}, u32[]{:S(2)}) copy-start(f32[16,256]{1,0:T(8,128)} %param.19) | copy-start | bytes 49156
  85.8 62.0 %copy-start.9 = (f32[16,256]{1,0:T(8,128)S(1)}, f32[16,256]{1,0:T(8,128)}, u32[]{:S(2)}) copy-start(f32[16,256]{1,0:T(8,128)} %param.17) | copy-start | bytes 49156
  85.8 62.0 %copy-start.10 = (f32[16,256]{1,0:T(8,128)S(1)}, f32[16,256]{1,0:T(8,128)}, u32[]{:S(2)}) copy-start(f32[16,256]{1,0:T(8,128)} %param.18) | copy-start | bytes 49156
  85.9 62.0 %copy-start.13 = (f32[256]{0:T(256)S(1)}, f32[256]{0:T(256)}, u32[]{:S(2)}) copy-start(f32[256]{0:T(256)} %param.13) | copy-start | bytes 3076
  142.8 128.9 %all-to-all-start = ((bf16[32,56,256]{2,1,0:T(8,128)(2,1)}), bf16[32,56,256]{2,1,0:T(8,128)(2,1)S(1)}, u32[]{:S(2)}, u32[]{:S(2)}) async-start(bf16[32,56,256]{2,1,0:T(8,128)(2,1)} %bitcast.2), calls=%async_computation | async-start | bytes 1835008 | tf_op jit(solution)/shard_map/all_to_all | solution.py:90
  147.7 198.7 %reduce-scatter.4.cloned.1.call-start = ((), (), s32[]{:S(2)}) async-start(), calls=%async_computation.5 | async-start | bytes 4571136
  270.5 2.0 copy-start.4
  270.5 2.0 copy-start.5
  270.5 246.7 %copy-start.1 = (bf16[512,256]{1,0:T(8,128)(2,1)}, bf16[512,256]{1,0:T(8,128)(2,1)S(1)}, u32[]{:S(2)}) copy-start(bf16[512,256]{1,0:T(8,128)(2,1)S(1)} %get-tuple-element.9) | copy-start | bytes 786436
  271.7 1.4 copy-start.2
  271.7 1.4 copy-start.3
  271.8 118.2 %copy-start.7 = (bf16[1,512,256]{2,1,0:T(8,128)(2,1)}, bf16[1,512,256]{2,1,0:T(8,128)(2,1)S(1)}, u32[]{:S(2)}) copy-start(bf16[1,512,256]{2,1,0:T(8,128)(2,1)S(1)} %get-tuple-element.12) | copy-start | bytes 786436
  272.5 0.9 copy-start.6
  281.8 108.2 %all-gather.2.cloned.1.call-start = ((), (), s32[]{:S(2)}) async-start(), calls=%async_computation.4 | async-start | bytes 2064384 | tf_op jit(solution)/shard_map/all_gather | solution.py:113
  393.1 23.6 %copy-start.12 = (f32[192,8]{0,1:T(8,128)S(1)}, f32[192,8]{0,1:T(8,128)}, u32[]{:S(2)}) copy-start(f32[192,8]{0,1:T(8,128)} %param.12) | copy-start | bytes 18436
  393.1 118.8 %all-to-all-start.2 = ((bf16[32,56,256]{2,1,0:T(8,128)(2,1)}), bf16[32,56,256]{2,1,0:T(8,128)(2,1)S(1)}, u32[]{:S(2)}, u32[]{:S(2)}) async-start(bf16[32,56,256]{2,1,0:T(8,128)(2,1)} %bitcast.8), calls=%async_computation.2 | async-start | bytes 1835008 | tf_op jit(solution)/shard_map/all_to_all | solution.py:121
Sparse Core Ops, SparseCore 0:
  281.9 64.3 reduce-scatter.3
  348.5 41.4 all-gather.1
where the time goes:
time: 526 us; the launch traced here: 525 us
  waiting for transfers between devices  242 us (46%)
  blocking collectives  149 us (28%)
  starting transfers between devices  74.8 us (14%)
  other arithmetic  23.3 us (4%)
  between operations  14.5 us (3%)
  local copies, waits for them, and re-layouts  12.8 us (2%)
  matrix products  8.01 us (2%)
    all_gather x1, blocking collectives, sent_together_2(): out, at, outs = (lax.all_gather(both, axis, axis=dim, tiled=True), 0, [])  123 us
    all_to_all x1, waiting for transfers between devices, per_device(): lax.all_to_all(produced.reshape(experts, capacity, portion_width), 'fs',...  80.7 us
    unnamed x3, waiting for transfers between devices  64.4 us
    all_to_all x1, waiting for transfers between devices, sent_together(): lax.all_to_all(both, axis, split_axis=split_dim, concat_axis=concat_dim,...  55.5 us
    all_to_all x1, starting transfers between devices, sent_together(): lax.all_to_all(both, axis, split_axis=split_dim, concat_axis=concat_dim,...  46.3 us
    all_gather x1, waiting for transfers between devices, per_device(): lax.all_gather((jax.nn.silu(gate_part) * up_part).astype(jnp.bfloat16), '...  41.7 us
    all_to_all x1, starting transfers between devices, per_device(): lax.all_to_all(produced.reshape(experts, capacity, portion_width), 'fs',...  23.3 us
    all_gather x1, blocking collectives, per_device(): lax.all_gather((jax.nn.silu(sgate_part) * sup_part).astype(jnp.bfloat16),...  13.4 us
  transfers between devices with their start and end apart: 5, of which 4 were waited for; matrix products, arithmetic and copies ran while one was open for 4% of the time, Pallas kernels for 0%

commit v1 on v0

--- a/solution.py
+++ b/solution.py
@@ -4,6 +4,12 @@
 from jax.sharding import PartitionSpec as P
 
 norm_eps = 1e-06
+
+
+def gather_by_exchange(x, axis, dim):
+    peers = lax.axis_size(axis)
+    repeats = [peers if d == dim else 1 for d in range(x.ndim)]
+    return lax.all_to_all(jnp.tile(x, repeats), axis, split_axis=dim, concat_axis=dim, tiled=True)
 
 
 def sent_together(arrays, axis, split_dim, concat_dim, along):
@@ -110,9 +116,7 @@
         )
     )
     hidden, shared_hidden = (
-        lax.all_gather(
-            (jax.nn.silu(gate_part) * up_part).astype(jnp.bfloat16), "tp", axis=1, tiled=True
-        ),
+        gather_by_exchange((jax.nn.silu(gate_part) * up_part).astype(jnp.bfloat16), "tp", 1),
         lax.all_gather(
             (jax.nn.silu(sgate_part) * sup_part).astype(jnp.bfloat16), "tp", axis=1, tiled=True
         ),

time: 526 us -> 509 us (0.968)
  waiting for transfers between devices: 242 us -> 200 us
  blocking collectives: 149 us -> 179 us
    all_gather x1 -> x0, waiting for transfers between devices: 41.7 us -> none  [per_device(): lax.all_gather((jax.nn.silu(gate_part) * up_part).astype(jnp.bfloat16), '...]
    all_to_all x0 -> x1, blocking collectives: none -> 28.6 us  [gather_by_exchange(): lax.all_to_all(jnp.tile(x, repeats), axis, split_axis=dim, concat_axis=di...]
    unnamed x3 -> x2, waiting for transfers between devices: 64.4 us -> 64.6 us
  transfers between devices with their start and end apart: 5 -> 4, of which waited for: 4 -> 3; matrix products, arithmetic and copies ran while one was open for 4% -> 4% of each run, Pallas kernels for 0% -> 0%
where the time goes in v1:
time: 509 us; the launch traced here: 508 us
  waiting for transfers between devices  200 us (39%)
  blocking collectives  179 us (35%)
  starting transfers between devices  73.3 us (14%)
  other arithmetic  22.6 us (4%)
  between operations  14.5 us (3%)
  local copies, waits for them, and re-layouts  12.9 us (3%)
  matrix products  6.46 us (1%)
    all_gather x1, blocking collectives, sent_together_2(): out, at, outs = (lax.all_gather(both, axis, axis=dim, tiled=True), 0, [])  123 us
    all_to_all x1, waiting for transfers between devices, per_device(): lax.all_to_all(produced.reshape(experts, capacity, portion_width), 'fs',...  79.5 us
    unnamed x2, waiting for transfers between devices  64.6 us
    all_to_all x1, waiting for transfers between devices, sent_together(): lax.all_to_all(both, axis, split_axis=split_dim, concat_axis=concat_dim,...  55.5 us
    all_to_all x1, starting transfers between devices, sent_together(): lax.all_to_all(both, axis, split_axis=split_dim, concat_axis=concat_dim,...  46.3 us
    all_to_all x1, blocking collectives, gather_by_exchange(): lax.all_to_all(jnp.tile(x, repeats), axis, split_axis=dim, concat_axis=di...  28.6 us
    all_to_all x1, starting transfers between devices, per_device(): lax.all_to_all(produced.reshape(experts, capacity, portion_width), 'fs',...  22.1 us
    all_gather x1, blocking collectives, per_device(): lax.all_gather((jax.nn.silu(sgate_part) * sup_part).astype(jnp.bfloat16),...  14.2 us
  transfers between devices with their start and end apart: 4, of which 3 were waited for; matrix products, arithmetic and copies ran while one was open for 4% of the time, Pallas kernels for 0%

profile of v1, /device:TPU:33, one launch (start us, length us, event | category | flops | bytes accessed | tf_op | source)
XLA Modules:
  0.0 508.0 jit_solution(9677543404593068625)
XLA Ops:
  7.2 1.1 convert_element_type.88
  8.3 1.3 multiply_convert_fusion.1
  9.6 1.0 pad_maximum_fusion.1
  10.6 46.3 %all-to-all-start.1 = ((bf16[32,16,768]{2,1,0:T(8,128)(2,1)}), bf16[32,16,768]{2,1,0:T(8,128)(2,1)S(1)}, u32[]{:S(2)}, u32[]{:S(2)}) async-start(bf16[32,16,768]{2,1,0:T(8,128)(2,1)} %pad_maximum_fusion.1), calls=%async_computation.1 | async-start | bytes 1572864 | tf_op jit(solution)/shard_map/all_to_all | solution.py:18
  57.3 9.1 %reduce-window.6 = s32[32,12,128]{2,1,0:T(8,128)S(1)} reduce-window(s32[32,12,128]{2,1,0:T(8,128)S(1)} %fusion.11, s32[]{:T(128)} %constant.6.clone.1), window={size=1x1x128 pad=0_0x0_0x127_0}, to_apply=%region_0.0 | reduce-window | flops 6242304 | bytes 393220 | tf_op jit(solution)/shard_map/reduce-window
  66.3 0.1 slice.38
  66.5 0.2 copy.48
  66.8 0.1 broadcast_add_fusion
  67.4 13.3 %psum.7 = f32[192]{0:T(256)S(1)} all-reduce(f32[192]{0:T(256)S(1)} %fusion.12), channel_id=1, replica_groups=mesh['grp'=2,'fs'=32,'tp'=8] {'tp'}, use_global_device_ids=true, to_apply=%region_5.6 | all-reduce | flops 192 | bytes 1536 | tf_op jit(solution)/shard_map/psum | solution.py:80
  80.8 5.1 convert_reduce_fusion
  85.9 1.4 convolution_convert_fusion.3
  87.3 55.5 %all-to-all-done.1 = bf16[32,16,768]{2,1,0:T(8,128)(2,1)S(1)} async-done(((bf16[32,16,768]{2,1,0:T(8,128)(2,1)}), bf16[32,16,768]{2,1,0:T(8,128)(2,1)S(1)}, u32[]{:S(2)}, u32[]{:S(2)}) %all-to-all-start.1) | async-done | bytes 786464 | tf_op jit(solution)/shard_map/all_to_all | solution.py:18
  142.8 4.8 all-to-all-start
  147.8 122.6 %all_gather.6 = bf16[512,768]{1,0:T(8,128)(2,1)S(1)} all-gather(bf16[16,768]{1,0:T(8,128)(2,1)S(1)} %pad_maximum_fusion.2), channel_id=1, replica_groups=mesh['grp'=2,'fs'=32,'tp'=8] {'fs'}, dimensions={0}, use_global_device_ids=true | all-gather | bytes 811008 | tf_op jit(solution)/shard_map/all_gather | solution.py:24
  270.5 0.2 convolution_convert_fusion.4
  270.7 0.9 convolution_convert_fusion.5
  271.8 0.7 convolution_convert_fusion
  272.5 0.7 convolution_convert_fusion.1
  273.2 0.2 copy-done.6
  273.4 2.1 pad_maximum_fusion
  275.4 6.3 %copy.57 = bf16[3968,512]{0,1:T(8,128)(2,1)} copy(bf16[3968,512]{1,0:T(8,128)(2,1)} %pad_maximum_fusion) | data formatting | bytes 8126464
  281.8 64.6 %reduce-scatter.4.cloned.1.call-done = bf16[64,3968]{1,0:T(8,128)(2,1)} async-done(((bf16[512,3968]{1,0:T(8,128)(2,1)}), bf16[64,3968]{1,0:T(8,128)(2,1)}) %reduce-scatter.4.cloned.1.call-update) | async-done | bytes 507920
  346.3 1.2 fusion.7
  347.7 28.6 %all_to_all.31 = bf16[1792,8,64]{0,2,1:T(8,128)(2,1)S(1)} all-to-all(bf16[1792,8,64]{0,2,1:T(8,128)(2,1)S(1)} %tile.2), channel_id=1, replica_groups=mesh['grp'=2,'fs'=32,'tp'=8] {'tp'}, dimensions={1} | all-to-all | bytes 3670016 | tf_op jit(solution)/shard_map/all_to_all | solution.py:12
  376.3 1.6 convolution_convert_fusion.2
  377.9 22.1 %all-to-all-start.3 = ((bf16[32,56,256]{2,1,0:T(8,128)(2,1)}), bf16[32,56,256]{2,1,0:T(8,128)(2,1)S(1)}, u32[]{:S(2)}, u32[]{:S(2)}) async-start(bf16[32,56,256]{2,1,0:T(8,128)(2,1)} %bitcast.9), calls=%async_computation.3 | async-start | bytes 1835008 | tf_op jit(solution)/shard_map/all_to_all | solution.py:125
  400.4 0.9 fusion.21
  401.3 14.2 %all_gather.7 = bf16[192,512]{0,1:T(8,128)(2,1)S(1)} all-gather(bf16[192,64]{0,1:T(8,128)(2,1)S(1)} %fusion.21), channel_id=1, replica_groups=mesh['grp'=2,'fs'=32,'tp'=8] {'tp'}, dimensions={1}, use_global_device_ids=true | all-gather | bytes 221184 | tf_op jit(solution)/shard_map/all_gather | solution.py:120
  415.5 79.5 %all-to-all-done.3 = bf16[32,56,256]{2,1,0:T(8,128)(2,1)S(1)} async-done(((bf16[32,56,256]{2,1,0:T(8,128)(2,1)}), bf16[32,56,256]{2,1,0:T(8,128)(2,1)S(1)}, u32[]{:S(2)}, u32[]{:S(2)}) %all-to-all-start.3) | async-done | bytes 917536 | tf_op jit(solution)/shard_map/all_to_all | solution.py:125
  495.0 4.8 gather_fusion
  499.7 0.5 fusion
  500.3 0.9 fusion.1
  (53 shorter events, 1.7 us)
Async XLA Ops:
  9.6 47.3 %copy-start.8 = (s32[192,8]{0,1:T(8,128)S(1)}, s32[192,8]{0,1:T(8,128)}, u32[]{:S(2)}) copy-start(s32[192,8]{0,1:T(8,128)} %param.11) | copy-start | bytes 18436
  10.6 132.3 %all-to-all-start.1 = ((bf16[32,16,768]{2,1,0:T(8,128)(2,1)}), bf16[32,16,768]{2,1,0:T(8,128)(2,1)S(1)}, u32[]{:S(2)}, u32[]{:S(2)}) async-start(bf16[32,16,768]{2,1,0:T(8,128)(2,1)} %pad_maximum_fusion.1), calls=%async_computation.1 | async-start | bytes 1572864 | tf_op jit(solution)/shard_map/all_to_all | solution.py:18
  56.9 10.4 %copy-start = (bf16[192,256]{1,0:T(8,128)(2,1)S(1)}, bf16[192,256]{1,0:T(8,128)(2,1)}, u32[]{:S(2)}) copy-start(bf16[192,256]{1,0:T(8,128)(2,1)} %param.10) | copy-start | bytes 294916
  85.8 61.9 %copy-start.11 = (f32[16,256]{1,0:T(8,128)S(1)}, f32[16,256]{1,0:T(8,128)}, u32[]{:S(2)}) copy-start(f32[16,256]{1,0:T(8,128)} %param.19) | copy-start | bytes 49156
  85.9 61.9 %copy-start.9 = (f32[16,256]{1,0:T(8,128)S(1)}, f32[16,256]{1,0:T(8,128)}, u32[]{:S(2)}) copy-start(f32[16,256]{1,0:T(8,128)} %param.17) | copy-start | bytes 49156
  85.9 61.9 %copy-start.10 = (f32[16,256]{1,0:T(8,128)S(1)}, f32[16,256]{1,0:T(8,128)}, u32[]{:S(2)}) copy-start(f32[16,256]{1,0:T(8,128)} %param.18) | copy-start | bytes 49156
  85.9 61.9 %copy-start.13 = (f32[256]{0:T(256)S(1)}, f32[256]{0:T(256)}, u32[]{:S(2)}) copy-start(f32[256]{0:T(256)} %param.13) | copy-start | bytes 3076
  142.8 128.9 %all-to-all-start = ((bf16[32,56,256]{2,1,0:T(8,128)(2,1)}), bf16[32,56,256]{2,1,0:T(8,128)(2,1)S(1)}, u32[]{:S(2)}, u32[]{:S(2)}) async-start(bf16[32,56,256]{2,1,0:T(8,128)(2,1)} %bitcast.2), calls=%async_computation | async-start | bytes 1835008 | tf_op jit(solution)/shard_map/all_to_all | solution.py:96
  147.7 198.7 %reduce-scatter.4.cloned.1.call-start = ((), (), s32[]{:S(2)}) async-start(), calls=%async_computation.5 | async-start | bytes 4571136
  270.4 2.0 copy-start.4
  270.4 2.0 copy-start.5
  270.5 229.8 %copy-start.1 = (bf16[512,256]{1,0:T(8,128)(2,1)}, bf16[512,256]{1,0:T(8,128)(2,1)S(1)}, u32[]{:S(2)}) copy-start(bf16[512,256]{1,0:T(8,128)(2,1)S(1)} %get-tuple-element.9) | copy-start | bytes 786436
  271.7 1.4 copy-start.2
  271.7 1.4 copy-start.3
  271.7 104.5 %copy-start.7 = (bf16[1,512,256]{2,1,0:T(8,128)(2,1)}, bf16[1,512,256]{2,1,0:T(8,128)(2,1)S(1)}, u32[]{:S(2)}) copy-start(bf16[1,512,256]{2,1,0:T(8,128)(2,1)S(1)} %get-tuple-element.12) | copy-start | bytes 786436
  272.5 0.9 copy-start.6
  377.9 22.4 %copy-start.12 = (f32[192,8]{0,1:T(8,128)S(1)}, f32[192,8]{0,1:T(8,128)}, u32[]{:S(2)}) copy-start(f32[192,8]{0,1:T(8,128)} %param.12) | copy-start | bytes 18436
  377.9 117.1 %all-to-all-start.3 = ((bf16[32,56,256]{2,1,0:T(8,128)(2,1)}), bf16[32,56,256]{2,1,0:T(8,128)(2,1)S(1)}, u32[]{:S(2)}, u32[]{:S(2)}) async-start(bf16[32,56,256]{2,1,0:T(8,128)(2,1)} %bitcast.9), calls=%async_computation.3 | async-start | bytes 1835008 | tf_op jit(solution)/shard_map/all_to_all | solution.py:125
Sparse Core Ops, SparseCore 0:
  281.9 64.3 reduce-scatter.3
